TPU v7x, 512 devices: a whole 4x8x8 slice. The times are simulated.
512 devices in a mesh: ep: 32 (over z, x), tp: 16 (over y, core).
Axes of the slice: x: 4, y: 8, z: 8, core: 2. Of those that a mesh axis runs over, the one named last changes fastest.
Arguments:
- mixer_query: bfloat16 [8192, 2048], P('ep', 'tp'), may hold values from -6 to 6
- mixer_forget: bfloat16 [8192, 2048], P('ep', 'tp'), may hold values from -5.5 to 5.5
- mixer_value: bfloat16 [8192, 2048], P('ep', 'tp'), may hold values from -6 to 6
- mixer_gate: bfloat16 [8192, 2048], P('ep', 'tp'), may hold values from -6 to 6
- forget_floor: float32 [2048], P('tp'), may hold values from 0.88 to 1
- head_gain: float32 [128], replicated, may hold values from 0.1 to 1.9
- mixer_proj: bfloat16 [2048, 2048], P(None, 'tp'), may hold values from -0.125 to 0.125
- expert_tokens: bfloat16 [4096, 2048], P('ep'), may hold values from -6 to 6
- expert_gain: float32 [2048], replicated, may hold values from 0.1 to 1.9
- routes: int32 [4096, 2], P('ep'), may hold values from 0 to 31, as said below
- group_logits: float32 [4096, 4], P('ep'), may hold values from -6 to 6
- choice_logits: float32 [4096, 2], P('ep'), may hold values from -6 to 6
- w_gate: bfloat16 [32, 2048, 2048], P('ep', None, 'tp'), may hold values from -0.125 to 0.125
- w_up: bfloat16 [32, 2048, 2048], P('ep', None, 'tp'), may hold values from -0.125 to 0.125
- w_down: bfloat16 [32, 2048, 2048], P('ep', None, 'tp'), may hold values from -0.125 to 0.125
Outputs:
- mixer_out: bfloat16 [8192, 2048], P('ep', 'tp')
- expert_out: bfloat16 [4096, 2048], P('ep', 'tp')
Inputs may be any that keep to these rules, and one draw needn't show every extreme that they name: `routes`: in each aligned block of 128 rows (the rows of one index of ep) no expert is named by more than 16 rows, and some expert reaches that bound in every block; the 2 experts of a row differ and lie in the same group.
All inputs are finite; a program needn't handle non-finite values.
Results may differ from a plain program's by a relative error of at most 0.01.
Values may be sent and summed in bfloat16 or wider, within the bound.
A program may use at most 64 MiB of HBM per device.

v0:
```python
import jax
import jax.numpy as jnp
from jax import lax
from jax.sharding import Mesh
from jax.sharding import PartitionSpec as P

KEYDIM = 128
VDIM = 128
GROUPS = 4
TOPK = 2
BLOCK = 64
EP = ("ep_0", "ep_1")
norm_eps = 1e-06
highest_precision = lax.Precision.HIGHEST


def filled_with(shard, identity):
    return jax.tree.map(
        lambda part, zero: jnp.zeros_like(part) + jnp.asarray(zero, part.dtype), shard, identity
    )


def collected_together(shard, axis):
    leaves = jax.tree.leaves(shard)
    sequence = sorted(range(len(leaves)), key=lambda k: -leaves[k].size)
    width = (1, *leaves[sequence[0]].shape)[-1]
    lines = [
        jnp.pad(leaves[k].reshape(-1), (0, -leaves[k].size % width)).reshape(-1, width)
        for k in sequence
    ]
    both, at, found = (lax.all_gather(jnp.concatenate(lines), axis), 0, {})
    for k, line in zip(sequence, lines):
        section = both[:, at : at + len(line)].reshape(len(both), -1)
        found[k] = section[:, : leaves[k].size].reshape(-1, *leaves[k].shape)
        at += len(line)
    numbers = iter(range(len(leaves)))
    return jax.tree.map(lambda _: found[next(numbers)], shard)


def carried_in(shard, axes, combine, identity):
    before = start = filled_with(shard, identity)
    so_far = shard
    for axis in reversed(axes):
        devices, index = (lax.axis_size(axis), lax.axis_index(axis))
        pieces = collected_together(
            jax.tree.map(
                lambda part, kind: part.astype(kind), so_far, (jnp.bfloat16, jnp.bfloat16)
            ),
            axis,
        )
        inside, so_far = (start, start)
        for k in range(devices):
            passed = k < index
            so_far = combine(
                so_far, jax.tree.map(lambda part, own: part[k].astype(own.dtype), pieces, shard)
            )
            inside = jax.tree.map(lambda new, old: jnp.where(passed, new, old), so_far, inside)
        before = combine(inside, before)
    return before


def laid_out(pieces, dim):
    dims = list(pieces.shape[1:])
    dims[dim] *= pieces.shape[0]
    return jnp.moveaxis(pieces, 0, dim).reshape(dims)


def from_everyone(shard, axis):
    copies = jnp.broadcast_to(shard, (lax.axis_size(axis), *shard.shape))
    return lax.all_to_all(copies, axis, split_axis=0, concat_axis=0, tiled=True)


def gather_directly(shard, axis, dim):
    return laid_out(from_everyone(shard, axis), dim)


def rms_scale(features, gain_vec):
    return (
        features
        * lax.rsqrt(jnp.mean(features * features, axis=-1, keepdims=True) + norm_eps)
        * gain_vec
    )


def block_terms(query_block, input_block, log_blk, value_block, carried_state):
    cumulative_log = jnp.cumsum(log_blk, axis=0)
    between_block_term = jnp.einsum(
        "zug,ugr->zur",
        query_block * jnp.exp(cumulative_log),
        carried_state,
        precision=highest_precision,
    )
    causal = jnp.tril(jnp.ones((query_block.shape[0], query_block.shape[0]), dtype=bool))[
        :, :, None, None
    ]
    differ = cumulative_log[:, None] - cumulative_log[None, :]
    decays = jnp.exp(jnp.where(causal, differ, -jnp.inf))
    scores = jnp.sum(query_block[:, None] * input_block[None, :] * decays, axis=-1)
    result = between_block_term + jnp.einsum(
        "tsh,shv->thv", scores, value_block, precision=highest_precision
    )
    ending_log_decay = cumulative_log[-1]
    updated_state = jnp.exp(ending_log_decay)[..., None] * carried_state + jnp.einsum(
        "twa,twr->war",
        input_block * jnp.exp(ending_log_decay[None] - cumulative_log),
        value_block,
        precision=highest_precision,
    )
    return (updated_state, result, cumulative_log)


def mixer_local(
    mixer_query, mixer_forget, mixer_value, mixer_gate, forget_floor, head_gain, mixer_proj
):
    length = mixer_query.shape[0]
    heads_local = mixer_query.shape[1] // KEYDIM
    blocks = length // BLOCK

    def split_blocks(source_array, last_width):
        return source_array.reshape(blocks, BLOCK, heads_local, last_width)

    queries = jax.nn.silu(mixer_query.astype(jnp.float32))
    input_rates = (1.0 - forget_floor) * jax.nn.sigmoid(-mixer_forget.astype(jnp.float32))
    log_forget = jnp.log1p(-input_rates)
    value_rows = mixer_value.astype(jnp.float32)

    def advance(carry_pair, block_inputs):
        carried_state, offset_log = carry_pair
        query_block, input_block, value_block, log_blk = block_inputs
        updated_state, result, cumulative_log = block_terms(
            query_block, input_block, log_blk, value_block, carried_state
        )
        scaled_values = query_block * jnp.exp(cumulative_log + offset_log[None])
        return ((updated_state, offset_log + cumulative_log[-1]), (result, scaled_values))

    initial = (
        jnp.zeros((heads_local, KEYDIM, VDIM), jnp.float32),
        jnp.zeros((heads_local, KEYDIM), jnp.float32),
    )
    (local_state, total_log), (output_rows, scaled_values) = lax.scan(
        advance,
        initial,
        (
            split_blocks(queries, KEYDIM),
            split_blocks(input_rates, KEYDIM),
            split_blocks(value_rows, VDIM),
            split_blocks(log_forget, KEYDIM),
        ),
    )

    def combine(earlier, later):
        return (earlier[0] * later[0], later[0][..., None] * earlier[1] + later[1])

    identity = (jnp.ones_like(total_log), jnp.zeros_like(local_state))
    incoming_state = carried_in((jnp.exp(total_log), local_state), EP, combine, identity)
    output_rows = output_rows + jnp.einsum(
        "qsfa,fap->qsfp", scaled_values, incoming_state[1], precision=highest_precision
    )
    output_rows = output_rows.reshape(length, heads_local, VDIM)
    gate_act = jax.nn.silu(mixer_gate.astype(jnp.float32)).reshape(length, heads_local, VDIM)
    gated_out = rms_scale(output_rows, head_gain) * gate_act
    mixed_heads = gated_out.reshape(length, heads_local * VDIM).astype(jnp.bfloat16)
    summed = jnp.dot(
        lax.all_gather(mixed_heads, "tp", axis=1, tiled=True),
        mixer_proj,
        preferred_element_type=jnp.float32,
    )
    return summed.astype(jnp.bfloat16)


def gate_weights(routes, group_logits, choice_logits, group_size):
    group_exp = jnp.exp(group_logits)
    group_prob = group_exp / jnp.sum(group_exp, axis=-1, keepdims=True)
    groups_of = routes // group_size
    member = (groups_of[..., None] == jnp.arange(GROUPS, dtype=jnp.int32)).astype(jnp.float32)
    picked_prob = jnp.sum(member * group_prob[:, None, :], axis=-1)
    choice_exp = jnp.exp(choice_logits)
    together = (groups_of[:, :, None] == groups_of[:, None, :]).astype(jnp.float32)
    within = jnp.sum(together * choice_exp[:, None, :], axis=-1)
    return picked_prob * choice_exp / within


def finish(gate_pre, up_pre, down_local, sources, slot_count):
    hidden = (jax.nn.silu(gate_pre) * up_pre).astype(jnp.bfloat16)
    summed = jnp.dot(
        gather_directly(hidden, "tp", 1), down_local, preferred_element_type=jnp.float32
    )
    shaped = summed.astype(jnp.bfloat16).reshape(sources, slot_count, down_local.shape[1])
    return lax.all_to_all(shaped, EP, split_axis=0, concat_axis=0, tiled=True)


def expert_local(
    expert_tokens, expert_gain, routes, group_logits, choice_logits, w_gate, w_up, w_down
):
    count_rows, model_width = expert_tokens.shape
    experts_all = lax.axis_size(EP)
    capacity = 2 * TOPK * count_rows // experts_all
    normed = rms_scale(expert_tokens.astype(jnp.float32), expert_gain).astype(jnp.bfloat16)
    weights = gate_weights(routes, group_logits, choice_logits, experts_all // GROUPS)
    flat_routes = routes.reshape(-1)
    onehot = (flat_routes[:, None] == jnp.arange(experts_all, dtype=jnp.int32)).astype(jnp.int32)
    earlier = jnp.cumsum(onehot, axis=0) - onehot
    ranks = jnp.sum(earlier * onehot, axis=-1)
    slot_of = flat_routes * capacity + ranks
    token_ids = jnp.arange(flat_routes.shape[0], dtype=jnp.int32) // TOPK
    token_of = jnp.full((experts_all * capacity,), count_rows, jnp.int32).at[slot_of].set(token_ids)
    padded = jnp.concatenate([normed, jnp.zeros((1, model_width), jnp.bfloat16)], axis=0)
    outgoing = padded[token_of].reshape(experts_all, capacity, model_width)
    gate_local = w_gate[0]
    up_local = w_up[0]
    down_local = w_down[0]
    arrived = lax.all_to_all(outgoing, EP, split_axis=0, concat_axis=0, tiled=True)
    sources, slot_count, _ = arrived.shape
    flat_in = arrived.reshape(sources * slot_count, model_width)
    gate_pre = jnp.dot(flat_in, gate_local, preferred_element_type=jnp.float32)
    up_pre = jnp.dot(flat_in, up_local, preferred_element_type=jnp.float32)
    came_back = finish(gate_pre, up_pre, down_local, sources, slot_count)
    picked = (
        came_back.reshape(-1, came_back.shape[-1])[slot_of].astype(jnp.float32)
        * weights.reshape(-1)[:, None]
    )
    return jnp.sum(picked.reshape(count_rows, TOPK, -1), axis=1).astype(jnp.bfloat16)


def per_device(
    mixer_query,
    mixer_forget,
    mixer_value,
    mixer_gate,
    forget_floor,
    head_gain,
    mixer_proj,
    expert_tokens,
    expert_gain,
    routes,
    group_logits,
    choice_logits,
    w_gate,
    w_up,
    w_down,
):
    mixer_out = mixer_local(
        mixer_query, mixer_forget, mixer_value, mixer_gate, forget_floor, head_gain, mixer_proj
    )
    expert_out = expert_local(
        expert_tokens, expert_gain, routes, group_logits, choice_logits, w_gate, w_up, w_down
    )
    return (mixer_out, expert_out)


def solution(mesh):
    finer = Mesh(mesh.devices.reshape(8, 4, mesh.shape["tp"]), ("ep_0", "ep_1", "tp"))
    placed = (
        P(EP, "tp"),
        P(EP, "tp"),
        P(EP, "tp"),
        P(EP, "tp"),
        P("tp"),
        P(),
        P(None, "tp"),
        P(EP, None),
        P(),
        P(EP, None),
        P(EP, None),
        P(EP, None),
        P(EP, None, "tp"),
        P(EP, None, "tp"),
        P(EP, None, "tp"),
    )
    return jax.shard_map(
        per_device,
        mesh=finer,
        in_specs=placed,
        out_specs=(P(EP, "tp"), P(EP, "tp")),
        check_vma=False,
    )
```

profile of v0, /device:TPU:1, one launch (start us, length us, event | category | flops | bytes accessed | tf_op | source)
XLA Modules:
  0.0 173.8 jit_solution(17011988294751444505)
XLA Ops:
  7.2 0.0 copy-start
  7.2 0.8 copy.50
  8.0 0.1 eq.55
  8.2 0.1 eq.51
  8.3 0.7 and_select_fusion
  9.0 0.6 reduce-window.6
  9.6 0.2 slice_reduce_fusion
  9.8 0.1 copy.49
  10.0 0.1 mul.434
  10.1 0.1 fusion.84
  10.2 1.4 scatter_custom_fusion
  11.6 1.2 fusion.24
  12.9 1.2 fusion.26
  14.2 3.3 %gather_fusion = bf16[512,2048]{1,0:T(8,128)(2,1)} fusion(bf16[129,2048]{1,0:T(8,128)(2,1)S(1)} %concatenate.11, s32[1024]{0:T(1024)S(1)} %pad_clamp_fusion.1), kind=kCustom, calls=%fused_computation | custom fusion | bytes 4196352 | tf_op jit(solution)/shard_map/gather | solution.py:208
  17.5 13.8 %all-to-all-start = ((bf16[32,16,2048]{2,1,0:T(8,128)(2,1)}), bf16[32,16,2048]{2,1,0:T(8,128)(2,1)S(1)}, u32[]{:S(2)}, u32[]{:S(2)}) async-start(bf16[32,16,2048]{2,1,0:T(8,128)(2,1)} %bitcast.31), calls=%async_computation | async-start | bytes 4194304 | tf_op jit(solution)/shard_map/all_to_all | solution.py:212
  31.5 0.1 divide_multiply_fusion
  31.6 13.7 %while.17 = (s32[]{:T(128)}, f32[1,128,128]{2,1,0:T(8,128)S(1)}, f32[1,128]{1,0:T(1,128)S(1)}, f32[4,64,1,128]{3,1,2,0:T(8,128)}, f32[4,64,1,128]{3,1,2,0:T(8,12...) while((s32[]{:T(128)}, f32[1,128,128]{2,1,0:T(8,128)S(1)}, ...), condition=%wide.region_3.4_spmd.clone, body=%wide.region_0.3_spmd.clone.sunk | while | flops 34709760 | bytes 1030797 | solution.py:140
  31.7 0.1 fusion.169
  31.8 0.6 multiply_dynamic-update-slice_fusion.2
  32.4 1.4 multiply_reduce_fusion.3
  33.7 0.2 convolution_bitcast_fusion.4
  34.0 0.8 fusion.173
  34.7 0.3 fusion.171
  35.1 0.1 fusion.169
  35.2 0.6 multiply_dynamic-update-slice_fusion.2
  35.8 1.4 multiply_reduce_fusion.3
  37.2 0.2 convolution_bitcast_fusion.4
  37.4 0.8 fusion.173
  38.2 0.3 fusion.171
  38.5 0.1 fusion.169
  38.6 0.6 multiply_dynamic-update-slice_fusion.2
  39.2 1.4 multiply_reduce_fusion.3
  40.6 0.2 convolution_bitcast_fusion.4
  40.8 0.8 fusion.173
  41.6 0.3 fusion.171
  41.9 0.1 fusion.169
  42.0 0.6 multiply_dynamic-update-slice_fusion.2
  42.7 1.4 multiply_reduce_fusion.3
  44.0 0.2 convolution_bitcast_fusion.4
  44.2 0.8 fusion.173
  45.0 0.3 fusion.171
  45.4 0.0 copy-start.9
  45.4 10.6 %all-gather.2 = bf16[4,129,128]{2,1,0:T(8,128)(2,1)S(1)} all-gather(bf16[1,129,128]{2,1,0:T(8,128)(2,1)S(1)} %maximum_bitcast_fusion), channel_id=2, replica_groups=mesh['ep_0'=8,'ep_1'=4,'tp'=16] {'ep_1'}, dimensions={0}, use_global_device_ids=true | all-gather | bytes 165120 | tf_op jit(solution)/shard_map/all_gather | solution.py:31
  56.0 23.8 %all-to-all-done = bf16[32,16,2048]{2,1,0:T(8,128)(2,1)S(1)} async-done(((bf16[32,16,2048]{2,1,0:T(8,128)(2,1)}), bf16[32,16,2048]{2,1,0:T(8,128)(2,1)S(1)}, u32[]{:S(2)}, u32[]{:S(2)}) %all-to-all-start) | async-done | bytes 2097184 | tf_op jit(solution)/shard_map/all_to_all | solution.py:212
  79.9 0.7 fusion.29
  80.6 0.7 fusion.22
  81.3 0.1 copy.53
  81.4 1.6 broadcast_in_dim.37
  83.0 9.9 %all-to-all-start.1 = ((bf16[16,512,128]{1,2,0:T(8,128)(2,1)}), bf16[16,512,128]{1,2,0:T(8,128)(2,1)S(1)}, u32[]{:S(2)}, u32[]{:S(2)}) async-start(bf16[16,512,128]{1,2,0:T(8,128)(2,1)} %broadcast_in_dim.37), calls=%async_computation.1 | async-start | bytes 4194304 | tf_op jit(solution)/shard_map/all_to_all | solution.py:70
  92.9 0.0 all-gather.6.cloned.1.call-start
  93.0 0.1 fusion.81
  93.1 20.6 %all-gather.3 = bf16[8,129,128]{2,1,0:T(8,128)(2,1)S(1)} all-gather(bf16[1,129,128]{2,1,0:T(8,128)(2,1)S(1)} %maximum_bitcast_fusion.1), channel_id=3, replica_groups=mesh['ep_0'=8,'ep_1'=4,'tp'=16] {'ep_0'}, dimensions={0}, use_global_device_ids=true | all-gather | bytes 297216 | tf_op jit(solution)/shard_map/all_gather | solution.py:31
  113.8 1.7 multiply_reduce_fusion.1
  115.5 0.1 rsqrt.20
  115.6 0.7 fusion.41
  116.3 0.0 all-gather.6.cloned.1.call-update
  116.4 0.1 copy.54
  116.6 26.2 %all-to-all-done.1 = bf16[16,512,128]{1,2,0:T(8,128)(2,1)S(1)} async-done(((bf16[16,512,128]{1,2,0:T(8,128)(2,1)}), bf16[16,512,128]{1,2,0:T(8,128)(2,1)S(1)}, u32[]{:S(2)}, u32[]{:S(2)}) %all-to-all-start.1) | async-done | bytes 2097184 | tf_op jit(solution)/shard_map/all_to_all | solution.py:70
  142.8 2.4 %convolution_convert_fusion = bf16[512,128]{1,0:T(8,128)(2,1)} fusion(bf16[512,2048]{0,1:T(8,128)(2,1)S(1)} %bitcast.225, bf16[1,2048,128]{2,1,0:T(8,128)(2,1)} %param.31), kind=kOutput, calls=%fused_computation.42 | convolution fusion | flops 268500992 | bytes 2752512 | tf_op jit(solution)/shard_map/dot_general | solution.py:185
  145.2 5.1 %all-to-all-start.2 = ((bf16[32,16,128]{2,1,0:T(8,128)(2,1)}), bf16[32,16,128]{2,1,0:T(8,128)(2,1)S(1)}, u32[]{:S(2)}, u32[]{:S(2)}) async-start(bf16[32,16,128]{2,1,0:T(8,128)(2,1)} %bitcast.38), calls=%async_computation.2 | async-start | bytes 262144 | tf_op jit(solution)/shard_map/all_to_all | solution.py:189
  150.3 12.6 %all-gather.6.cloned.1.call-done = bf16[256,2048]{1,0:T(8,128)(2,1)} async-done(((bf16[256,128]{1,0:T(8,128)(2,1)}), bf16[256,2048]{1,0:T(8,128)(2,1)}) %all-gather.6.cloned.1.call-update) | async-done | bytes 1048592 | tf_op jit(solution)/shard_map/all_gather | solution.py:164
  162.9 2.3 %convolution_convert_fusion.1 = bf16[256,128]{1,0:T(8,128)(2,1)} fusion(bf16[256,2048]{1,0:T(8,128)(2,1)} %all-gather.6.cloned.1.call-done, bf16[2048,128]{1,0:T(8,128)(2,1)S(1)} %copy-done.1), kind=kOutput, calls=%fused_computation.45 | convolution fusion | flops 134250496 | bytes 1638400 | tf_op jit(solution)/shard_map/dot_general | solution.py:163
  165.2 0.9 gather_fusion.1
  166.1 0.9 fusion.38
  (82 shorter events, 0.6 us)
Async XLA Ops:
  7.2 72.7 %copy-start = (bf16[1,2048,128]{2,1,0:T(8,128)(2,1)S(1)}, bf16[1,2048,128]{2,1,0:T(8,128)(2,1)}, u32[]{:S(2)}) copy-start(bf16[1,2048,128]{2,1,0:T(8,128)(2,1)} %param.29) | copy-start | bytes 1572868
  17.5 13.9 %copy-start.10 = (f32[128]{0:T(128)S(1)}, f32[128]{0:T(128)}, u32[]{:S(2)}) copy-start(f32[128]{0:T(128)} %param.21) | copy-start | bytes 1540
  17.5 13.9 %copy-start.2 = (bf16[256,128]{1,0:T(8,128)(2,1)S(1)}, bf16[256,128]{1,0:T(8,128)(2,1)}, u32[]{:S(2)}) copy-start(bf16[256,128]{1,0:T(8,128)(2,1)} %param.19) | copy-start | bytes 196612
  17.5 14.0 %copy-start.3 = (bf16[256,128]{1,0:T(8,128)(2,1)S(1)}, bf16[256,128]{1,0:T(8,128)(2,1)}, u32[]{:S(2)}) copy-start(bf16[256,128]{1,0:T(8,128)(2,1)} %param.17) | copy-start | bytes 196612
  17.5 14.0 %copy-start.4 = (bf16[256,128]{1,0:T(8,128)(2,1)S(1)}, bf16[256,128]{1,0:T(8,128)(2,1)}, u32[]{:S(2)}) copy-start(bf16[256,128]{1,0:T(8,128)(2,1)} %param.18) | copy-start | bytes 196612
  17.5 62.3 %all-to-all-start = ((bf16[32,16,2048]{2,1,0:T(8,128)(2,1)}), bf16[32,16,2048]{2,1,0:T(8,128)(2,1)S(1)}, u32[]{:S(2)}, u32[]{:S(2)}) async-start(bf16[32,16,2048]{2,1,0:T(8,128)(2,1)} %bitcast.31), calls=%async_computation | async-start | bytes 4194304 | tf_op jit(solution)/shard_map/all_to_all | solution.py:212
  45.4 35.2 %copy-start.9 = (bf16[1,2048,128]{2,1,0:T(8,128)(2,1)S(1)}, bf16[1,2048,128]{2,1,0:T(8,128)(2,1)}, u32[]{:S(2)}) copy-start(bf16[1,2048,128]{2,1,0:T(8,128)(2,1)} %param.30) | copy-start | bytes 1572868
  83.0 32.6 %copy-start.5 = (bf16[256,128]{1,0:T(8,128)(2,1)S(1)}, bf16[256,128]{1,0:T(8,128)(2,1)}, u32[]{:S(2)}) copy-start(bf16[256,128]{1,0:T(8,128)(2,1)} %param.20) | copy-start | bytes 196612
  83.0 32.6 %copy-start.8 = (f32[128]{0:T(128)S(1)}, f32[128]{0:T(128)}, u32[]{:S(2)}) copy-start(f32[128]{0:T(128)} %param.22) | copy-start | bytes 1540
  83.0 59.8 %all-to-all-start.1 = ((bf16[16,512,128]{1,2,0:T(8,128)(2,1)}), bf16[16,512,128]{1,2,0:T(8,128)(2,1)S(1)}, u32[]{:S(2)}, u32[]{:S(2)}) async-start(bf16[16,512,128]{1,2,0:T(8,128)(2,1)} %broadcast_in_dim.37), calls=%async_computation.1 | async-start | bytes 4194304 | tf_op jit(solution)/shard_map/all_to_all | solution.py:70
  92.9 23.5 %copy-start.7 = (f32[128,2]{0,1:T(2,128)S(1)}, f32[128,2]{0,1:T(2,128)}, u32[]{:S(2)}) copy-start(f32[128,2]{0,1:T(2,128)} %param.28) | copy-start | bytes 3076
  92.9 23.5 %copy-start.6 = (f32[128,4]{0,1:T(4,128)S(1)}, f32[128,4]{0,1:T(4,128)}, u32[]{:S(2)}) copy-start(f32[128,4]{0,1:T(4,128)} %param.27) | copy-start | bytes 6148
  92.9 70.0 %all-gather.6.cloned.1.call-start = ((), (), s32[]{:S(2)}) async-start(), calls=%async_computation.3 | async-start | bytes 1114112 | tf_op jit(solution)/shard_map/all_gather | solution.py:164
  113.8 49.2 %copy-start.1 = (bf16[2048,128]{1,0:T(8,128)(2,1)S(1)}, bf16[2048,128]{1,0:T(8,128)(2,1)}, u32[]{:S(2)}) copy-start(bf16[2048,128]{1,0:T(8,128)(2,1)} %param.23) | copy-start | bytes 1572868
  145.2 20.0 %all-to-all-start.2 = ((bf16[32,16,128]{2,1,0:T(8,128)(2,1)}), bf16[32,16,128]{2,1,0:T(8,128)(2,1)S(1)}, u32[]{:S(2)}, u32[]{:S(2)}) async-start(bf16[32,16,128]{2,1,0:T(8,128)(2,1)} %bitcast.38), calls=%async_computation.2 | async-start | bytes 262144 | tf_op jit(solution)/shard_map/all_to_all | solution.py:189
Sparse Core Ops, SparseCore 0:
  116.4 46.4 all-gather.5
where the time goes:
time: 174 us
  waiting for transfers between devices  62.6 us (36%)
  blocking collectives  31.2 us (18%)
  starting transfers between devices  28.9 us (17%)
  between operations  14.4 us (8%)
  other arithmetic  14.2 us (8%)
  matrix products  12.9 us (7%)
  local copies, waits for them, and re-layouts  9.24 us (5%)
    all_gather x2, blocking collectives, collected_together(): both, at, found = (lax.all_gather(jnp.concatenate(lines), axis), 0, {})  31.2 us
    all_to_all x1, waiting for transfers between devices, from_everyone(): return lax.all_to_all(copies, axis, split_axis=0, concat_axis=0, tiled=True)  26.2 us
    all_to_all x1, waiting for transfers between devices, expert_local(): lax.all_to_all(outgoing, EP, split_axis=0, concat_axis=0, tiled=True)  23.8 us
    all_to_all x1, starting transfers between devices, expert_local(): lax.all_to_all(outgoing, EP, split_axis=0, concat_axis=0, tiled=True)  13.8 us
    all_gather x1, waiting for transfers between devices, mixer_local(): lax.all_gather(mixed_heads, 'tp', axis=1, tiled=True)  12.6 us
    all_to_all x1, starting transfers between devices, from_everyone(): return lax.all_to_all(copies, axis, split_axis=0, concat_axis=0, tiled=True)  9.89 us
    reduce_sum x4, other arithmetic, block_terms(): jnp.sum(query_block[:, None] * input_block[None, :] * decays, axis=-1)  5.4 us
    all_to_all x1, starting transfers between devices, finish(): return lax.all_to_all(shaped, EP, split_axis=0, concat_axis=0, tiled=True)  5.08 us
  transfers between devices with their start and end apart: 4, of which 3 were waited for; matrix products, arithmetic and copies ran while one was open for 12% of the time, Pallas kernels for 0%

commit v1 on v0

--- a/solution.py
+++ b/solution.py
@@ -161,7 +161,9 @@
     gated_out = rms_scale(output_rows, head_gain) * gate_act
     mixed_heads = gated_out.reshape(length, heads_local * VDIM).astype(jnp.bfloat16)
     summed = jnp.dot(
-        lax.all_gather(mixed_heads, "tp", axis=1, tiled=True),
+        jnp.concatenate(
+            lax.all_to_all(jnp.stack([mixed_heads] * lax.axis_size("tp")), "tp", 0, 0), axis=1
+        ),
         mixer_proj,
         preferred_element_type=jnp.float32,
     )

time: 174 us -> 189 us (1.086)
  waiting for transfers between devices: 62.6 us -> 89.2 us
  between operations: 14.4 us -> 1.04 us
  starting transfers between devices: 28.9 us -> 35.3 us
  matrix products: 12.9 us -> 9.52 us
  other arithmetic: 14.2 us -> 11.2 us
    all_to_all x0 -> x1, waiting for transfers between devices: none -> 25.4 us  [mixer_local(): lax.all_to_all(jnp.stack([mixed_heads] * lax.axis_size('tp')), 'tp', 0, 0)]
    all_to_all x1, waiting for transfers between devices: 23.8 us -> 48.2 us  [expert_local(): lax.all_to_all(outgoing, EP, split_axis=0, concat_axis=0, tiled=True)]
    all_to_all x1, waiting for transfers between devices: 26.2 us -> 7.94 us  [from_everyone(): return lax.all_to_all(copies, axis, split_axis=0, concat_axis=0, tiled=True)]
    all_gather x1 -> x0, waiting for transfers between devices: 12.6 us -> none  [mixer_local(): lax.all_gather(mixed_heads, 'tp', axis=1, tiled=True)]
    all_to_all x1, waiting for transfers between devices: 0.01 us -> 7.69 us  [finish(): return lax.all_to_all(shaped, EP, split_axis=0, concat_axis=0, tiled=True)]
    all_to_all x0 -> x1, starting transfers between devices: none -> 5.78 us  [mixer_local(): lax.all_to_all(jnp.stack([mixed_heads] * lax.axis_size('tp')), 'tp', 0, 0)]
    dot_general x4, matrix products: 3.09 us -> 0.66 us  [block_terms(): jnp.einsum('tsh,shv->thv', scores, value_block, precision=highest_precision)]
    dynamic_update_slice x4, other arithmetic: 2.49 us -> 0.07 us  [mixer_local(): lax.scan(advance, initial, (split_blocks(queries, KEYDIM), split_blocks(i...]
  transfers between devices with their start and end apart: 4 -> 4, of which waited for: 3 -> 4; matrix products, arithmetic and copies ran while one was open for 12% -> 8% of each run, Pallas kernels for 0% -> 0%
where the time goes in v1:
time: 189 us; the launch traced here: 188 us
  waiting for transfers between devices  89.2 us (47%)
  starting transfers between devices  35.3 us (19%)
  blocking collectives  30.8 us (16%)
  other arithmetic  11.2 us (6%)
  local copies, waits for them, and re-layouts  10.9 us (6%)
  matrix products  9.52 us (5%)
    all_to_all x1, waiting for transfers between devices, expert_local(): lax.all_to_all(outgoing, EP, split_axis=0, concat_axis=0, tiled=True)  48.2 us
    all_gather x2, blocking collectives, collected_together(): both, at, found = (lax.all_gather(jnp.concatenate(lines), axis), 0, {})  30.8 us
    all_to_all x1, waiting for transfers between devices, mixer_local(): lax.all_to_all(jnp.stack([mixed_heads] * lax.axis_size('tp')), 'tp', 0, 0)  25.4 us
    all_to_all x1, starting transfers between devices, expert_local(): lax.all_to_all(outgoing, EP, split_axis=0, concat_axis=0, tiled=True)  13.8 us
    all_to_all x1, starting transfers between devices, from_everyone(): return lax.all_to_all(copies, axis, split_axis=0, concat_axis=0, tiled=True)  9.89 us
    all_to_all x1, waiting for transfers between devices, from_everyone(): return lax.all_to_all(copies, axis, split_axis=0, concat_axis=0, tiled=True)  7.94 us
    all_to_all x1, waiting for transfers between devices, finish(): return lax.all_to_all(shaped, EP, split_axis=0, concat_axis=0, tiled=True)  7.69 us
    all_to_all x1, starting transfers between devices, mixer_local(): lax.all_to_all(jnp.stack([mixed_heads] * lax.axis_size('tp')), 'tp', 0, 0)  5.78 us
  transfers between devices with their start and end apart: 4, of which 4 were waited for; matrix products, arithmetic and copies ran while one was open for 8% of the time, Pallas kernels for 0%

profile of v1, /device:TPU:1, one launch (start us, length us, event | category | flops | bytes accessed | tf_op | source)
XLA Modules:
  0.0 188.3 jit_solution(12842501978591698539)
XLA Ops:
  0.6 0.0 copy-start
  0.6 0.8 copy.53
  1.5 0.1 eq.55
  1.6 0.1 eq.51
  1.8 0.7 and_select_fusion
  2.5 0.6 reduce-window.6
  3.1 0.2 slice_reduce_fusion
  3.3 0.1 copy.52
  3.4 0.1 mul.434
  3.6 0.1 fusion.84
  3.7 1.4 scatter_custom_fusion
  5.1 1.2 fusion.24
  6.3 1.2 fusion.26
  7.6 3.3 %gather_fusion = bf16[512,2048]{1,0:T(8,128)(2,1)} fusion(bf16[129,2048]{1,0:T(8,128)(2,1)S(1)} %concatenate.11, s32[1024]{0:T(1024)S(1)} %pad_clamp_fusion.1), kind=kCustom, calls=%fused_computation | custom fusion | bytes 4196352 | tf_op jit(solution)/shard_map/gather | solution.py:210
  11.0 13.8 %all-to-all-start.1 = ((bf16[32,16,2048]{2,1,0:T(8,128)(2,1)}), bf16[32,16,2048]{2,1,0:T(8,128)(2,1)S(1)}, u32[]{:S(2)}, u32[]{:S(2)}) async-start(bf16[32,16,2048]{2,1,0:T(8,128)(2,1)} %bitcast.33), calls=%async_computation.1 | async-start | bytes 4194304 | tf_op jit(solution)/shard_map/all_to_all | solution.py:214
  25.0 0.1 divide_multiply_fusion
  25.1 48.2 %all-to-all-done.1 = bf16[32,16,2048]{2,1,0:T(8,128)(2,1)S(1)} async-done(((bf16[32,16,2048]{2,1,0:T(8,128)(2,1)}), bf16[32,16,2048]{2,1,0:T(8,128)(2,1)S(1)}, u32[]{:S(2)}, u32[]{:S(2)}) %all-to-all-start.1) | async-done | bytes 2097184 | tf_op jit(solution)/shard_map/all_to_all | solution.py:214
  73.3 0.7 fusion.29
  74.0 0.3 copy-done.9
  74.4 0.7 fusion.22
  75.1 0.1 copy.56
  75.2 1.6 broadcast_in_dim.37
  76.8 9.9 %all-to-all-start.2 = ((bf16[16,512,128]{1,2,0:T(8,128)(2,1)}), bf16[16,512,128]{1,2,0:T(8,128)(2,1)S(1)}, u32[]{:S(2)}, u32[]{:S(2)}) async-start(bf16[16,512,128]{1,2,0:T(8,128)(2,1)} %broadcast_in_dim.37), calls=%async_computation.2 | async-start | bytes 4194304 | tf_op jit(solution)/shard_map/all_to_all | solution.py:70
  86.7 9.0 %while.17 = (s32[]{:T(128)}, f32[1,128,128]{2,1,0:T(8,128)S(1)}, f32[1,128]{1,0:T(1,128)S(1)}, f32[4,64,1,128]{3,1,2,0:T(8,128)S(1)}, f32[4,64,1,128]{3,1,2,0:T(...) while((s32[]{:T(128)}, f32[1,128,128]{2,1,0:T(8,128)S(1)}, ...), condition=%wide.region_3.4_spmd.clone, body=%wide.region_0.3_spmd.clone.sunk | while | flops 34709760 | bytes 1046165 | solution.py:140
  86.7 0.1 fusion.169
  86.8 1.4 multiply_reduce_fusion.3
  88.2 0.2 convolution_bitcast_fusion.4
  88.4 0.2 fusion.173
  88.6 0.3 fusion.171
  89.0 0.1 fusion.169
  89.1 1.4 multiply_reduce_fusion.3
  90.5 0.2 convolution_bitcast_fusion.4
  90.7 0.2 fusion.173
  90.9 0.3 fusion.171
  91.2 0.1 fusion.169
  91.4 1.4 multiply_reduce_fusion.3
  92.7 0.2 convolution_bitcast_fusion.4
  92.9 0.2 fusion.173
  93.1 0.3 fusion.171
  93.5 0.1 fusion.169
  93.6 1.4 multiply_reduce_fusion.3
  95.0 0.2 convolution_bitcast_fusion.4
  95.2 0.2 fusion.173
  95.4 0.3 fusion.171
  95.7 0.0 copy-start.5
  95.7 0.0 copy-start.8
  95.8 10.2 %all-gather.2 = bf16[4,129,128]{2,1,0:T(8,128)(2,1)S(1)} all-gather(bf16[1,129,128]{2,1,0:T(8,128)(2,1)S(1)} %maximum_bitcast_fusion), channel_id=2, replica_groups=mesh['ep_0'=8,'ep_1'=4,'tp'=16] {'ep_1'}, dimensions={0}, use_global_device_ids=true | all-gather | bytes 165120 | tf_op jit(solution)/shard_map/all_gather | solution.py:31
  106.1 0.1 fusion.81
  106.2 20.5 %all-gather.3 = bf16[8,129,128]{2,1,0:T(8,128)(2,1)S(1)} all-gather(bf16[1,129,128]{2,1,0:T(8,128)(2,1)S(1)} %maximum_bitcast_fusion.1), channel_id=3, replica_groups=mesh['ep_0'=8,'ep_1'=4,'tp'=16] {'ep_0'}, dimensions={0}, use_global_device_ids=true | all-gather | bytes 297216 | tf_op jit(solution)/shard_map/all_gather | solution.py:31
  126.8 0.7 multiply_reduce_fusion.1
  127.5 0.1 rsqrt.20
  127.5 0.1 fusion.41
  127.7 0.1 copy.51
  127.8 7.9 %all-to-all-done.2 = bf16[16,512,128]{1,2,0:T(8,128)(2,1)S(1)} async-done(((bf16[16,512,128]{1,2,0:T(8,128)(2,1)}), bf16[16,512,128]{1,2,0:T(8,128)(2,1)S(1)}, u32[]{:S(2)}, u32[]{:S(2)}) %all-to-all-start.2) | async-done | bytes 2097184 | tf_op jit(solution)/shard_map/all_to_all | solution.py:70
  135.7 1.1 stack.2
  136.8 5.8 %all-to-all-start = ((bf16[16,256,128]{1,2,0:T(8,128)(2,1)}), bf16[16,256,128]{1,2,0:T(8,128)(2,1)}, u32[]{:S(2)}, u32[]{:S(2)}) async-start(bf16[16,256,128]{1,2,0:T(8,128)(2,1)} %stack.2), calls=%async_computation | async-start | bytes 2097152 | tf_op jit(solution)/shard_map/all_to_all | solution.py:165
  142.7 0.1 copy.57
  142.9 2.5 %convolution_convert_fusion = bf16[512,128]{1,0:T(8,128)(2,1)} fusion(bf16[512,2048]{0,1:T(8,128)(2,1)S(1)} %bitcast.226, bf16[1,2048,128]{2,1,0:T(8,128)(2,1)} %param.31), kind=kOutput, calls=%fused_computation.42 | convolution fusion | flops 268500992 | bytes 2752512 | tf_op jit(solution)/shard_map/dot_general | solution.py:187
  145.3 25.4 %all-to-all-done = bf16[16,256,128]{1,2,0:T(8,128)(2,1)} async-done(((bf16[16,256,128]{1,2,0:T(8,128)(2,1)}), bf16[16,256,128]{1,2,0:T(8,128)(2,1)}, u32[]{:S(2)}, u32[]{:S(2)}) %all-to-all-start) | async-done | bytes 1048608 | tf_op jit(solution)/shard_map/all_to_all | solution.py:165
  170.7 5.8 %all-to-all-start.3 = ((bf16[32,16,128]{2,1,0:T(8,128)(2,1)}), bf16[32,16,128]{2,1,0:T(8,128)(2,1)S(1)}, u32[]{:S(2)}, u32[]{:S(2)}) async-start(bf16[32,16,128]{2,1,0:T(8,128)(2,1)} %bitcast.40), calls=%async_computation.3 | async-start | bytes 262144 | tf_op jit(solution)/shard_map/all_to_all | solution.py:191
  176.5 2.3 %convolution_convert_fusion.1 = bf16[256,128]{1,0:T(8,128)(2,1)} fusion(bf16[256,2048]{0,1:T(8,128)(2,1)} %bitcast.29, bf16[2048,128]{1,0:T(8,128)(2,1)S(1)} %copy-done.1), kind=kOutput, calls=%fused_computation.45 | convolution fusion | flops 134250496 | bytes 1638400 | tf_op jit(solution)/shard_map/dot_general | solution.py:163
  178.9 7.7 %all-to-all-done.3 = bf16[32,16,128]{2,1,0:T(8,128)(2,1)S(1)} async-done(((bf16[32,16,128]{2,1,0:T(8,128)(2,1)}), bf16[32,16,128]{2,1,0:T(8,128)(2,1)S(1)}, u32[]{:S(2)}, u32[]{:S(2)}) %all-to-all-start.3) | async-done | bytes 131104 | tf_op jit(solution)/shard_map/all_to_all | solution.py:191
  186.6 0.9 gather_fusion.1
  187.4 0.9 fusion.38
  (85 shorter events, 0.7 us)
Async XLA Ops:
  0.6 72.7 %copy-start = (bf16[1,2048,128]{2,1,0:T(8,128)(2,1)S(1)}, bf16[1,2048,128]{2,1,0:T(8,128)(2,1)}, u32[]{:S(2)}) copy-start(bf16[1,2048,128]{2,1,0:T(8,128)(2,1)} %param.29) | copy-start | bytes 1572868
  11.0 13.9 %copy-start.2 = (bf16[256,128]{1,0:T(8,128)(2,1)S(1)}, bf16[256,128]{1,0:T(8,128)(2,1)}, u32[]{:S(2)}) copy-start(bf16[256,128]{1,0:T(8,128)(2,1)} %param.19) | copy-start | bytes 196612
  11.0 13.9 %copy-start.11 = (f32[128]{0:T(128)S(1)}, f32[128]{0:T(128)}, u32[]{:S(2)}) copy-start(f32[128]{0:T(128)} %param.21) | copy-start | bytes 1540
  11.0 14.0 %copy-start.3 = (bf16[256,128]{1,0:T(8,128)(2,1)S(1)}, bf16[256,128]{1,0:T(8,128)(2,1)}, u32[]{:S(2)}) copy-start(bf16[256,128]{1,0:T(8,128)(2,1)} %param.17) | copy-start | bytes 196612
  11.0 14.0 %copy-start.4 = (bf16[256,128]{1,0:T(8,128)(2,1)S(1)}, bf16[256,128]{1,0:T(8,128)(2,1)}, u32[]{:S(2)}) copy-start(bf16[256,128]{1,0:T(8,128)(2,1)} %param.18) | copy-start | bytes 196612
  11.0 62.3 %all-to-all-start.1 = ((bf16[32,16,2048]{2,1,0:T(8,128)(2,1)}), bf16[32,16,2048]{2,1,0:T(8,128)(2,1)S(1)}, u32[]{:S(2)}, u32[]{:S(2)}) async-start(bf16[32,16,2048]{2,1,0:T(8,128)(2,1)} %bitcast.33), calls=%async_computation.1 | async-start | bytes 4194304 | tf_op jit(solution)/shard_map/all_to_all | solution.py:214
  73.3 1.0 copy-start.9
  76.8 9.9 %copy-start.10 = (f32[4,64,1,128]{3,1,2,0:T(8,128)S(1)}, f32[4,64,1,128]{3,1,2,0:T(8,128)}, u32[]{:S(2)}) copy-start(f32[4,64,1,128]{3,1,2,0:T(8,128)} %custom-call.7) | copy-start | bytes 393220
  76.8 58.9 %all-to-all-start.2 = ((bf16[16,512,128]{1,2,0:T(8,128)(2,1)}), bf16[16,512,128]{1,2,0:T(8,128)(2,1)S(1)}, u32[]{:S(2)}, u32[]{:S(2)}) async-start(bf16[16,512,128]{1,2,0:T(8,128)(2,1)} %broadcast_in_dim.37), calls=%async_computation.2 | async-start | bytes 4194304 | tf_op jit(solution)/shard_map/all_to_all | solution.py:70
  95.7 31.8 %copy-start.5 = (bf16[256,128]{1,0:T(8,128)(2,1)S(1)}, bf16[256,128]{1,0:T(8,128)(2,1)}, u32[]{:S(2)}) copy-start(bf16[256,128]{1,0:T(8,128)(2,1)} %param.20) | copy-start | bytes 196612
  95.7 31.8 %copy-start.8 = (f32[128]{0:T(128)S(1)}, f32[128]{0:T(128)}, u32[]{:S(2)}) copy-start(f32[128]{0:T(128)} %param.22) | copy-start | bytes 1540
  127.4 15.2 %copy-start.7 = (f32[128,2]{0,1:T(2,128)S(1)}, f32[128,2]{0,1:T(2,128)}, u32[]{:S(2)}) copy-start(f32[128,2]{0,1:T(2,128)} %param.28) | copy-start | bytes 3076
  127.4 15.2 %copy-start.6 = (f32[128,4]{0,1:T(4,128)S(1)}, f32[128,4]{0,1:T(4,128)}, u32[]{:S(2)}) copy-start(f32[128,4]{0,1:T(4,128)} %param.27) | copy-start | bytes 6148
  136.8 39.7 %copy-start.1 = (bf16[2048,128]{1,0:T(8,128)(2,1)S(1)}, bf16[2048,128]{1,0:T(8,128)(2,1)}, u32[]{:S(2)}) copy-start(bf16[2048,128]{1,0:T(8,128)(2,1)} %param.23) | copy-start | bytes 1572868
  136.8 33.9 %all-to-all-start = ((bf16[16,256,128]{1,2,0:T(8,128)(2,1)}), bf16[16,256,128]{1,2,0:T(8,128)(2,1)}, u32[]{:S(2)}, u32[]{:S(2)}) async-start(bf16[16,256,128]{1,2,0:T(8,128)(2,1)} %stack.2), calls=%async_computation | async-start | bytes 2097152 | tf_op jit(solution)/shard_map/all_to_all | solution.py:165
  170.7 15.8 %all-to-all-start.3 = ((bf16[32,16,128]{2,1,0:T(8,128)(2,1)}), bf16[32,16,128]{2,1,0:T(8,128)(2,1)S(1)}, u32[]{:S(2)}, u32[]{:S(2)}) async-start(bf16[32,16,128]{2,1,0:T(8,128)(2,1)} %bitcast.40), calls=%async_computation.3 | async-start | bytes 262144 | tf_op jit(solution)/shard_map/all_to_all | solution.py:191
